TPU v7x, 32 devices: a whole 2x2x4 slice. The times are simulated.
32 devices in a mesh: sp: 8 (over z, y), tp: 4 (over x, core).
Axes of the slice: x: 2, y: 2, z: 4, core: 2. Of those that a mesh axis runs over, the one named last changes fastest.
Arguments:
- stream: bfloat16 [1024, 2048], P('sp', 'tp'), may hold values from -40 to 40
- queries: bfloat16 [1024, 1024], P('sp', 'tp'), may hold values from -6 to 6
- keys: bfloat16 [1024, 1024], P('sp', 'tp'), may hold values from -6 to 6
- values: bfloat16 [1024, 2048], P('sp', 'tp'), may hold values from -25 to 25
- out_gate: bfloat16 [1024, 2048], P('sp', 'tp'), may hold values from -8 to 8
- input_gate: float32 [1024, 8], P('sp', 'tp'), may hold values from -9 to 350
- forget_gate: float32 [1024, 8], P('sp', 'tp'), may hold values from -4 to 20
- head_gain: float32 [2048], P('tp'), may hold values from 0.1 to 1.9
- w_out: bfloat16 [2048, 2048], P('tp'), may hold values from -0.125 to 0.125
- ffn_gain: float32 [2048], replicated, may hold values from 0.1 to 1.9
- w_gate: bfloat16 [2048, 5632], P('sp', 'tp'), may hold values from -0.125 to 0.125
- w_up: bfloat16 [2048, 5632], P('sp', 'tp'), may hold values from -0.125 to 0.125
- w_down: bfloat16 [5632, 2048], P('tp', 'sp'), may hold values from -0.078125 to 0.078125
Outputs:
- mixed: bfloat16 [1024, 2048], P('sp', 'tp')
All inputs are finite; a program needn't handle non-finite values.
Results may differ from a plain program's by a relative error of at most 0.0095.
Values may be sent and summed in bfloat16 or wider, within the bound.
No kernel may reach another device: no remote copies, remote signals or barrier semaphores. Data moves between devices by JAX's collectives and lax.ppermute only.
A program may use at most 128 MiB of HBM per device.

v0:
```python
import jax
import jax.numpy as jnp
from jax import lax
from jax.sharding import PartitionSpec as P

D = 2048
DQK = 128
DV = 256
BLOCK = 64
VALS = 2048
precise = lax.Precision.HIGHEST
norm_eps = 1e-06
very_low = -1e30


def entering(value, axis, join, neutral):
    count, mine = (lax.axis_size(axis), lax.axis_index(axis))
    pieces = jax.tree.map(lambda part: lax.all_gather(part, axis), value)
    subtotal = jax.tree.map(
        lambda part, zero: jnp.full_like(part, 0) + jnp.asarray(zero, part.dtype), value, neutral
    )

    def step(position, subtotal):
        longer = join(subtotal, jax.tree.map(lambda part: part[position], pieces))
        return jax.tree.map(lambda new, old: jnp.where(position < mine, new, old), longer, subtotal)

    return lax.fori_loop(0, count - 1, step, subtotal)


def block_summary(key_blk, value_blk, input_blk, decay_sum):
    decay_total = decay_sum[..., -1]
    log_weight = decay_total[..., None] - decay_sum + input_blk
    weight_peak = jnp.max(log_weight, axis=-1)
    weights = jnp.exp(log_weight - weight_peak[..., None])
    state_mat = jnp.einsum(
        "...ld,...le->...de", weights[..., None] * key_blk, value_blk, precision=precise
    )
    state_vec = jnp.einsum("...l,...ld->...d", weights, key_blk, precision=precise)
    return (state_mat, state_vec, weight_peak, decay_total)


def combine(earlier, later):
    ceiling = jnp.maximum(later[3] + earlier[2], later[2])
    former = jnp.exp(later[3] + earlier[2] - ceiling)
    latter = jnp.exp(later[2] - ceiling)
    return (
        former[..., None, None] * earlier[0] + latter[..., None, None] * later[0],
        former[..., None] * earlier[1] + latter[..., None] * later[1],
        ceiling,
        earlier[3] + later[3],
    )


def block_output(
    query_blk, key_blk, value_blk, input_blk, decay_sum, state_mat, state_vec, state_peak
):
    block_len = query_blk.shape[-2]
    causal = jnp.tril(jnp.ones((block_len, block_len), jnp.bool_))
    log_pair = jnp.where(
        causal,
        decay_sum[..., :, None] - decay_sum[..., None, :] + input_blk[..., None, :],
        -jnp.inf,
    )
    log_carry = decay_sum + state_peak[..., None]
    row_peak = jnp.maximum(log_carry, jnp.max(log_pair, axis=-1))
    scores = jnp.einsum("...ld,...sd->...ls", query_blk, key_blk, precision=precise) * jnp.exp(
        log_pair - row_peak[..., None]
    )
    carried = jnp.exp(log_carry - row_peak)
    numer = jnp.einsum("...ls,...se->...le", scores, value_blk, precision=precise) + carried[
        ..., None
    ] * jnp.einsum("...ld,...de->...le", query_blk, state_mat, precision=precise)
    normer = jnp.sum(scores, axis=-1) + carried * jnp.einsum(
        "...ld,...d->...l", query_blk, state_vec, precision=precise
    )
    denom = jnp.maximum(jnp.abs(normer), jnp.exp(-row_peak))
    return numer / denom[..., None]


def local(
    stream,
    queries,
    keys,
    values,
    out_gate,
    input_gate,
    forget_gate,
    head_gain,
    w_out,
    ffn_gain,
    w_gate,
    w_up,
    w_down,
):
    gate_full, up_full, down_full = (
        lax.all_gather(w_gate, "sp", axis=0, tiled=True),
        lax.all_gather(w_up, "sp", axis=0, tiled=True),
        lax.all_gather(w_down, "sp", axis=1, tiled=True),
    )
    count_of_rows = stream.shape[0]
    head_count = input_gate.shape[1]
    blocks = count_of_rows // BLOCK

    def to_blocks(array, col_width):
        return (
            array.astype(jnp.float32)
            .reshape(blocks, BLOCK, head_count, col_width)
            .transpose(2, 0, 1, 3)
        )

    query_blk = to_blocks(queries, DQK) * DQK ** (-0.5)
    key_blk = to_blocks(keys, DQK)
    value_blk = to_blocks(values, DV)
    input_blk = input_gate.reshape(blocks, BLOCK, head_count).transpose(2, 0, 1)
    decay_sum = jnp.cumsum(
        jax.nn.log_sigmoid(forget_gate).reshape(blocks, BLOCK, head_count).transpose(2, 0, 1),
        axis=-1,
    )
    summary = block_summary(key_blk, value_blk, input_blk, decay_sum)
    identity = (
        jnp.zeros((head_count, DQK, DV), jnp.float32),
        jnp.zeros((head_count, DQK), jnp.float32),
        jnp.full((head_count,), very_low, jnp.float32),
        jnp.zeros((head_count,), jnp.float32),
    )

    def advance(carry, piece):
        return (combine(carry, piece), carry)

    local_total, prefix = lax.scan(
        advance, identity, jax.tree.map(lambda array: jnp.moveaxis(array, 1, 0), summary)
    )
    carry_in = entering(local_total, "sp", combine, identity)
    start = combine(
        jax.tree.map(lambda array: array[:, None], carry_in),
        jax.tree.map(lambda array: jnp.moveaxis(array, 0, 1), prefix),
    )
    mixed_heads = block_output(
        query_blk, key_blk, value_blk, input_blk, decay_sum, start[0], start[1], start[2]
    )
    head_rows = mixed_heads.transpose(1, 2, 0, 3).reshape(count_of_rows, head_count, DV)
    local_sq = jnp.sum(head_rows * head_rows, axis=(1, 2))
    total_sq = lax.psum(local_sq, "tp")
    row_scale = lax.rsqrt(total_sq / VALS + norm_eps)
    gated = (
        head_rows
        * row_scale[:, None, None]
        * head_gain.reshape(head_count, DV)
        * jax.nn.sigmoid(out_gate.astype(jnp.float32).reshape(count_of_rows, head_count, DV))
    )
    heads_out = gated.reshape(count_of_rows, head_count * DV).astype(jnp.bfloat16)
    partial_value = jnp.dot(heads_out, w_out, preferred_element_type=jnp.float32)
    col_width = stream.shape[1]
    col_start = lax.axis_index("tp") * col_width
    mixer_own = lax.psum_scatter(
        partial_value.astype(jnp.bfloat16), "tp", scatter_dimension=1, tiled=True
    ).astype(jnp.float32)
    resid_own = (stream.astype(jnp.float32) + mixer_own).astype(jnp.bfloat16)
    resid_f = resid_own.astype(jnp.float32)
    square_total = lax.psum(jnp.sum(resid_f * resid_f, axis=-1), "tp")
    gain_own = lax.dynamic_slice_in_dim(ffn_gain, col_start, col_width)
    normed_own = (resid_f * lax.rsqrt(square_total / D + norm_eps)[:, None] * gain_own).astype(
        jnp.bfloat16
    )
    normed = lax.all_gather(normed_own, "tp", axis=1, tiled=True)
    gate_act = jnp.dot(normed, gate_full, preferred_element_type=jnp.float32)
    up_act = jnp.dot(normed, up_full, preferred_element_type=jnp.float32)
    hidden = (jax.nn.silu(gate_act) * up_act).astype(jnp.bfloat16)
    term = jnp.dot(hidden, down_full, preferred_element_type=jnp.float32)
    down_own = lax.psum_scatter(
        term.astype(jnp.bfloat16), "tp", scatter_dimension=1, tiled=True
    ).astype(jnp.float32)
    return (resid_own.astype(jnp.float32) + down_own).astype(jnp.bfloat16)


def solution(mesh):
    in_specs = (
        P("sp", "tp"),
        P("sp", "tp"),
        P("sp", "tp"),
        P("sp", "tp"),
        P("sp", "tp"),
        P("sp", "tp"),
        P("sp", "tp"),
        P("tp"),
        P("tp", None),
        P(),
        P("sp", "tp"),
        P("sp", "tp"),
        P("tp", "sp"),
    )
    out_specs = P("sp", "tp")
    return jax.shard_map(local, mesh=mesh, in_specs=in_specs, out_specs=out_specs, check_vma=False)
```

profile of v0, /device:TPU:0, one launch (start us, length us, event | category | flops | bytes accessed | tf_op | source)
XLA Modules:
  0.0 422.1 jit_solution(10034435100602329406)
XLA Ops:
  6.6 0.8 fusion.59
  8.2 0.8 reshape.66
  9.2 0.9 reshape.64
  10.0 0.9 reshape.67
  11.8 2.2 while.43
  16.5 23.2 %all-reduce.2 = (f32[16]{0:T(128)S(1)}, f32[16]{0:T(128)S(1)}) all-reduce(f32[16]{0:T(128)S(1)} %dynamic-update-slice, f32[16]{0:T(128)S(1)} %dynamic-update-slice.1), channel_id=2, replica_groups=mesh['sp'=8,'tp'=4] {'sp'}, use_global_device_ids=true, to_apply=%add | all-reduce | flops 32 | bytes 256
  40.0 16.7 %all-gather.4 = f32[8,2,128]{2,1,0:T(2,128)S(1)} all-gather(f32[1,2,128]{2,1,0:T(2,128)S(1)} %bitcast.218), channel_id=5, replica_groups=mesh['sp'=8,'tp'=4] {'sp'}, dimensions={0}, use_global_device_ids=true | all-gather | bytes 9216 | tf_op jit(solution)/shard_map/all_gather | solution.py:18
  56.8 10.0 %all-gather.16.cloned.1.call-done = f32[16,128,256]{2,1,0:T(8,128)} async-done(((f32[2,128,256]{2,1,0:T(8,128)}), f32[16,128,256]{2,1,0:T(8,128)}) %all-gather.16.cloned.1.call-update) | async-done | bytes 2097168 | tf_op jit(solution)/shard_map/all_gather | solution.py:18
  66.8 8.3 %while.44 = (s32[]{:T(128)}, f32[2,128,256]{2,1,0:T(8,128)S(1)}, f32[2,128]{1,0:T(2,128)S(1)}, f32[2]{0:T(128)S(1)}, s32[]{:T(128)}, /*index=5*/f32[8,2]{1,0:T(8...) while((s32[]{:T(128)}, f32[2,128,256]{2,1,0:T(8,128)S(1)}, ...), condition=%wide.region_5.6_spmd.clone, body=%wide.region_4.5_spmd.clone.sunk | while | flops 328978 | bytes 789757 | solution.py:27
  66.9 1.1 fusion.87
  68.1 1.1 fusion.87
  69.2 1.1 fusion.87
  70.4 1.1 fusion.87
  71.6 1.1 fusion.87
  72.8 1.1 fusion.87
  74.0 1.1 fusion.87
  76.5 1.7 multiply_reduce_fusion
  78.5 5.6 %psum.14 = f32[128]{0:T(128)S(1)} all-reduce(f32[128]{0:T(128)S(1)} %reduce_sum.34), channel_id=1, replica_groups=mesh['sp'=8,'tp'=4] {'tp'}, use_global_device_ids=true, to_apply=%region_9.10 | all-reduce | flops 128 | bytes 1024 | tf_op jit(solution)/shard_map/psum | solution.py:143
  84.2 1.3 convolution_convert_fusion
  87.5 0.8 dynamic_slice.46
  88.2 17.9 %reduce-scatter.3.cloned.1.call-done = bf16[128,512]{1,0:T(8,128)(2,1)} async-done(((bf16[128,2048]{1,0:T(8,128)(2,1)}), bf16[128,512]{1,0:T(8,128)(2,1)}) %reduce-scatter.3.cloned.1.call-update) | async-done | bytes 131088 | tf_op jit(solution)/shard_map/reduce_scatter | solution.py:155
  106.1 1.0 fusion.25
  107.1 5.8 %psum.15 = f32[128]{0:T(128)S(1)} all-reduce(f32[128]{0:T(128)S(1)} %fusion.25), channel_id=1, replica_groups=mesh['sp'=8,'tp'=4] {'tp'}, use_global_device_ids=true, to_apply=%region_12.13 | all-reduce | flops 128 | bytes 1024 | tf_op jit(solution)/shard_map/psum | solution.py:160
  112.9 1.0 fusion.27
  113.9 6.9 %all_gather.44 = bf16[128,2048]{1,0:T(8,128)(2,1)S(1)} all-gather(bf16[128,512]{1,0:T(8,128)(2,1)S(1)} %fusion.27), channel_id=1, replica_groups=mesh['sp'=8,'tp'=4] {'tp'}, dimensions={1}, use_global_device_ids=true | all-gather | bytes 655360 | tf_op jit(solution)/shard_map/all_gather | solution.py:165
  120.8 79.9 %all-gather.10.cloned.1.call-done = bf16[2048,1408]{1,0:T(8,128)(2,1)} async-done(((bf16[256,1408]{1,0:T(8,128)(2,1)}), bf16[2048,1408]{1,0:T(8,128)(2,1)}) %all-gather.10.cloned.1.call-update) | async-done | bytes 5767184 | tf_op jit(solution)/shard_map/all_gather | solution.py:96
  200.7 4.5 %fusion.68 = f32[128,1408]{1,0:T(8,128)} fusion(bf16[128,2048]{1,0:T(8,128)(2,1)S(1)} %all_gather.44, bf16[2048,1408]{1,0:T(8,128)(2,1)} %all-gather.10.cloned.1.call-done), kind=kOutput, calls=%fused_computation.119 | convolution fusion | flops 738197504 | bytes 7012352 | tf_op jit(solution)/shard_map/dot_general | solution.py:166
  205.2 88.0 %all-gather.12.cloned.1.call-done = bf16[2048,1408]{1,0:T(8,128)(2,1)} async-done(((bf16[256,1408]{1,0:T(8,128)(2,1)}), bf16[2048,1408]{1,0:T(8,128)(2,1)}) %all-gather.12.cloned.1.call-update) | async-done | bytes 5767184 | tf_op jit(solution)/shard_map/all_gather | solution.py:97
  293.2 93.2 %all-gather.14.cloned.1.call-done = bf16[1408,2048]{1,0:T(8,128)(2,1)} async-done(((bf16[1408,256]{1,0:T(8,128)(2,1)}), bf16[1408,2048]{1,0:T(8,128)(2,1)}) %all-gather.14.cloned.1.call-update) | async-done | bytes 5767184 | tf_op jit(solution)/shard_map/all_gather | solution.py:98
  386.5 7.2 %convolution_convert_fusion.1 = bf16[128,2048]{1,0:T(8,128)(2,1)} fusion(bf16[1408,2048]{1,0:T(8,128)(2,1)} %all-gather.14.cloned.1.call-done, bf16[128,2048]{1,0:T(8,128)(2,1)S(1)} %all_gather.44, bf16[2048,1408]{1,0:T(8,128)(2,1)} %all-gather.12.cloned.1.call-done, f32[128,1408]{1,0:T(8,128)} %fusion.68), kind=kOutput, calls=%fused_computation.40 | convolution fusion | flops 1477738496 | bytes 13303808 | tf_op jit(solution)/shard_map/dot_general | solution.py:169
  393.7 20.0 %reduce-scatter.5.cloned.1.call-done = bf16[128,512]{1,0:T(8,128)(2,1)} async-done(((bf16[128,2048]{1,0:T(8,128)(2,1)}), bf16[128,512]{1,0:T(8,128)(2,1)}) %reduce-scatter.5.cloned.1.call-update) | async-done | bytes 131088 | tf_op jit(solution)/shard_map/reduce_scatter | solution.py:170
  413.7 1.6 fusion.28
  (115 shorter events, 10.5 us)
Async XLA Ops:
  6.5 77.6 %copy-start = (bf16[512,2048]{1,0:T(8,128)(2,1)S(1)}, bf16[512,2048]{1,0:T(8,128)(2,1)}, u32[]{:S(2)}) copy-start(bf16[512,2048]{1,0:T(8,128)(2,1)} %param.25) | copy-start | bytes 6291460
  6.5 8.3 %copy-start.7 = (u32[32]{0:T(128)S(1)}, u32[32]{0:T(128)}, u32[]{:S(2)}) copy-start(u32[32]{0:T(128)} %constant.93) | copy-start | bytes 388
  6.5 33.4 %copy-start.4 = (bf16[128,256]{1,0:T(8,128)(2,1)S(1)}, bf16[128,256]{1,0:T(8,128)(2,1)}, u32[]{:S(2)}) copy-start(bf16[128,256]{1,0:T(8,128)(2,1)} %param.18) | copy-start | bytes 196612
  6.5 60.3 %all-gather.16.cloned.1.call-start = ((), (), s32[]{:S(2)}) async-start(), calls=%async_computation.7 | async-start | bytes 2359296 | tf_op jit(solution)/shard_map/all_gather | solution.py:18
  14.0 0.7 copy-start.1
  14.0 70.2 %copy-start.5 = (bf16[128,512]{1,0:T(8,128)(2,1)S(1)}, bf16[128,512]{1,0:T(8,128)(2,1)}, u32[]{:S(2)}) copy-start(bf16[128,512]{1,0:T(8,128)(2,1)} %param.21) | copy-start | bytes 393220
  14.0 70.1 %copy-start.6 = (f32[512]{0:T(512)S(1)}, f32[512]{0:T(512)}, u32[]{:S(2)}) copy-start(f32[512]{0:T(512)} %param.24) | copy-start | bytes 6148
  14.7 91.4 %reduce-scatter.3.cloned.1.call-start = ((), (), s32[]{:S(2)}) async-start(), calls=%async_computation.2 | async-start | bytes 655360 | tf_op jit(solution)/shard_map/reduce_scatter | solution.py:155
  75.1 31.0 %copy-start.2 = (bf16[128,512]{1,0:T(8,128)(2,1)S(1)}, bf16[128,512]{1,0:T(8,128)(2,1)}, u32[]{:S(2)}) copy-start(bf16[128,512]{1,0:T(8,128)(2,1)} %param.17) | copy-start | bytes 393220
  85.5 115.2 %all-gather.10.cloned.1.call-start = ((), (), s32[]{:S(2)}) async-start(), calls=%async_computation.3 | async-start | bytes 6488064 | tf_op jit(solution)/shard_map/all_gather | solution.py:96
  86.2 207.0 %all-gather.12.cloned.1.call-start = ((), (), s32[]{:S(2)}) async-start(), calls=%async_computation.4 | async-start | bytes 6488064 | tf_op jit(solution)/shard_map/all_gather | solution.py:97
  86.8 299.6 %all-gather.14.cloned.1.call-start = ((), (), s32[]{:S(2)}) async-start(), calls=%async_computation.5 | async-start | bytes 6488064 | tf_op jit(solution)/shard_map/all_gather | solution.py:98
  87.4 326.3 %reduce-scatter.5.cloned.1.call-start = ((), (), s32[]{:S(2)}) async-start(), calls=%async_computation.6 | async-start | bytes 655360 | tf_op jit(solution)/shard_map/reduce_scatter | solution.py:170
  205.2 208.5 %copy-start.3 = (bf16[128,512]{1,0:T(8,128)(2,1)S(1)}, bf16[128,512]{1,0:T(8,128)(2,1)}, u32[]{:S(2)}) copy-start(bf16[128,512]{1,0:T(8,128)(2,1)} %reduce-scatter.3.cloned.1.call-done) | copy-start | bytes 393220
Sparse Core Ops, SparseCore 0:
  14.9 51.9 all-gather.15
  85.6 20.4 reduce-scatter.2
  108.3 92.3 all-gather.9
  202.7 90.4 all-gather.11
  295.1 91.2 all-gather.13
  393.8 19.7 reduce-scatter.4
where the time goes:
time: 423 us; the launch traced here: 422 us
  waiting for transfers between devices  311 us (74%)
  blocking collectives  58.2 us (14%)
  matrix products  16.3 us (4%)
  other arithmetic  15.8 us (4%)
  between operations  14.4 us (3%)
  local copies, waits for them, and re-layouts  6.37 us (2%)
    all_gather x1, waiting for transfers between devices, local(): lax.all_gather(w_down, 'sp', axis=1, tiled=True)  93.2 us
    all_gather x1, waiting for transfers between devices, local(): lax.all_gather(w_up, 'sp', axis=0, tiled=True)  88 us
    all_gather x1, waiting for transfers between devices, local(): lax.all_gather(w_gate, 'sp', axis=0, tiled=True)  79.9 us
    unnamed x1, blocking collectives  23.2 us
    reduce_scatter x1, waiting for transfers between devices, local(): lax.psum_scatter(term.astype(jnp.bfloat16), 'tp', scatter_dimension=1, ti...  20 us
    reduce_scatter x1, waiting for transfers between devices, local(): lax.psum_scatter(partial_value.astype(jnp.bfloat16), 'tp', scatter_dimens...  17.9 us
    all_gather x1, blocking collectives, entering(): pieces = jax.tree.map(lambda part: lax.all_gather(part, axis), value)  16.7 us
    all_gather x1, waiting for transfers between devices, entering(): pieces = jax.tree.map(lambda part: lax.all_gather(part, axis), value)  10 us
  transfers between devices with their start and end apart: 6, of which 6 were waited for; matrix products, arithmetic and copies ran while one was open for 2% of the time, Pallas kernels for 0%

commit v1 on v0

--- a/solution.py
+++ b/solution.py
@@ -11,6 +11,17 @@
 precise = lax.Precision.HIGHEST
 norm_eps = 1e-06
 very_low = -1e30
+
+
+def ring_gather(array, axis, dim):
+    ways = lax.axis_size(axis)
+    pieces = [array]
+    for far in range(1, ways):
+        pieces.append(
+            lax.ppermute(pieces[far - 1], axis, [(d, (d - 1) % ways) for d in range(ways)])
+        )
+    line = jnp.concatenate(pieces, axis=dim)
+    return jnp.roll(line, lax.axis_index(axis) * array.shape[dim], axis=dim)
 
 
 def entering(value, axis, join, neutral):
@@ -93,7 +104,7 @@
     w_down,
 ):
     gate_full, up_full, down_full = (
-        lax.all_gather(w_gate, "sp", axis=0, tiled=True),
+        ring_gather(w_gate, "sp", 0),
         lax.all_gather(w_up, "sp", axis=0, tiled=True),
         lax.all_gather(w_down, "sp", axis=1, tiled=True),
     )

time: 423 us -> 424 us (level)
  waiting for transfers between devices: 311 us -> 218 us
  local copies, waits for them, and re-layouts: 6.37 us -> 42 us
  starting transfers between devices: 0.2 us -> 33.1 us
  other arithmetic: 15.8 us -> 35.8 us
    ppermute x0 -> x7, waiting for transfers between devices: none -> 138 us  [ring_gather(): lax.ppermute(pieces[far - 1], axis, [(d, (d - 1) % ways) for d in range(w...]
    all_gather x1, waiting for transfers between devices: 88 us -> 0.01 us  [local(): lax.all_gather(w_up, 'sp', axis=0, tiled=True)]
    all_gather x1 -> x0, waiting for transfers between devices: 79.9 us -> none  [local(): lax.all_gather(w_gate, 'sp', axis=0, tiled=True)]
    all_gather x1, waiting for transfers between devices: 93.2 us -> 51.8 us  [local(): lax.all_gather(w_down, 'sp', axis=1, tiled=True)]
    ppermute x0 -> x7, starting transfers between devices: none -> 33 us  [ring_gather(): lax.ppermute(pieces[far - 1], axis, [(d, (d - 1) % ways) for d in range(w...]
    unnamed x24 -> x43, local copies, waits for them, and re-layouts: 1.95 us -> 28.7 us
    reduce_scatter x1, waiting for transfers between devices: 17.9 us -> 0.01 us  [local(): lax.psum_scatter(partial_value.astype(jnp.bfloat16), 'tp', scatter_dimens...]
    select_n x21, other arithmetic: 8.15 us -> 16.9 us  [step(): jnp.where(position < mine, new, old)]
  transfers between devices with their start and end apart: 6 -> 12, of which waited for: 6 -> 10; matrix products, arithmetic and copies ran while one was open for 2% -> 9% of each run, Pallas kernels for 0% -> 0%
where the time goes in v1:
time: 424 us; the launch traced here: 422 us
  waiting for transfers between devices  218 us (51%)
  blocking collectives  59.3 us (14%)
  local copies, waits for them, and re-layouts  42 us (10%)
  other arithmetic  35.8 us (8%)
  starting transfers between devices  33.1 us (8%)
  matrix products  19.4 us (5%)
  between operations  14 us (3%)
    ppermute x7, waiting for transfers between devices, ring_gather(): lax.ppermute(pieces[far - 1], axis, [(d, (d - 1) % ways) for d in range(w...  138 us
    all_gather x1, waiting for transfers between devices, local(): lax.all_gather(w_down, 'sp', axis=1, tiled=True)  51.8 us
    ppermute x7, starting transfers between devices, ring_gather(): lax.ppermute(pieces[far - 1], axis, [(d, (d - 1) % ways) for d in range(w...  33 us
    unnamed x43, local copies, waits for them, and re-layouts  28.7 us
    unnamed x1, blocking collectives  23.2 us
    reduce_scatter x1, waiting for transfers between devices, local(): lax.psum_scatter(term.astype(jnp.bfloat16), 'tp', scatter_dimension=1, ti...  20 us
    select_n x21, other arithmetic, step(): jnp.where(position < mine, new, old)  16.9 us
    all_gather x1, blocking collectives, entering(): pieces = jax.tree.map(lambda part: lax.all_gather(part, axis), value)  16.6 us
  transfers between devices with their start and end apart: 12, of which 10 were waited for; matrix products, arithmetic and copies ran while one was open for 9% of the time, Pallas kernels for 0%

profile of v1, /device:TPU:0, one launch (start us, length us, event | category | flops | bytes accessed | tf_op | source)
XLA Modules:
  0.0 422.1 jit_solution(7951234977871233525)
XLA Ops:
  11.8 8.1 %while.43 = (s32[]{:T(128)}, f32[2,128,256]{2,1,0:T(8,128)S(1)}, f32[2,128]{1,0:T(2,128)S(1)}, f32[2]{0:T(128)S(1)}, f32[2]{0:T(128)S(1)}, /*index=5*/f32[2,2,12...) while((s32[]{:T(128)}, f32[2,128,256]{2,1,0:T(8,128)S(1)}, ...), condition=%wide.region_3.4_spmd.clone, body=%wide.region_2.3_spmd.clone.sunk | while | flops 328979 | bytes 1317212 | solution.py:141
  23.0 23.2 %all-reduce.2 = (f32[16]{0:T(128)S(1)}, f32[16]{0:T(128)S(1)}) all-reduce(f32[16]{0:T(128)S(1)} %dynamic-update-slice, f32[16]{0:T(128)S(1)} %dynamic-update-slice.1), channel_id=2, replica_groups=mesh['sp'=8,'tp'=4] {'sp'}, use_global_device_ids=true, to_apply=%add | all-reduce | flops 32 | bytes 256
  48.5 16.6 %all-gather.4 = f32[8,2,128]{2,1,0:T(2,128)S(1)} all-gather(f32[1,2,128]{2,1,0:T(2,128)S(1)} %bitcast.217), channel_id=5, replica_groups=mesh['sp'=8,'tp'=4] {'sp'}, dimensions={0}, use_global_device_ids=true | all-gather | bytes 9216 | tf_op jit(solution)/shard_map/all_gather | solution.py:29
  65.3 7.4 %all-gather.13.cloned.1.call-done = f32[16,128,256]{2,1,0:T(8,128)} async-done(((f32[2,128,256]{2,1,0:T(8,128)}), f32[16,128,256]{2,1,0:T(8,128)}) %all-gather.13.cloned.1.call-update) | async-done | bytes 2097168 | tf_op jit(solution)/shard_map/all_gather | solution.py:29
  72.7 21.7 %while.44 = (s32[]{:T(128)}, f32[2,128,256]{2,1,0:T(8,128)S(1)}, f32[2,128]{1,0:T(2,128)S(1)}, f32[2]{0:T(128)}, s32[]{:T(128)}, /*index=5*/f32[8,2]{1,0:T(8,128...) while((s32[]{:T(128)}, f32[2,128,256]{2,1,0:T(8,128)S(1)}, ...), condition=%wide.region_5.6_spmd.clone, body=%wide.region_4.5_spmd.clone.sunk | while | flops 328978 | bytes 789757 | solution.py:38
  105.0 5.6 %psum.14 = f32[128]{0:T(128)S(1)} all-reduce(f32[128]{0:T(128)S(1)} %reduce_sum.34), channel_id=1, replica_groups=mesh['sp'=8,'tp'=4] {'tp'}, use_global_device_ids=true, to_apply=%region_9.10 | all-reduce | flops 128 | bytes 1024 | tf_op jit(solution)/shard_map/psum | solution.py:154
  110.7 2.2 convolution_convert_fusion
  114.3 2.3 collective-permute-start
  116.6 15.6 %collective-permute-done = bf16[256,1408]{1,0:T(8,128)(2,1)S(1)} collective-permute-done((bf16[256,1408]{1,0:T(8,128)(2,1)S(1)}, bf16[256,1408]{1,0:T(8,128)(2,1)S(1)}, u32[]{:S(2)}, u32[]{:S(2)}) %collective-permute-start) | collective-permute-done | bytes 720928 | tf_op jit(solution)/shard_map/ppermute | solution.py:21
  132.2 4.6 %collective-permute-start.1 = (bf16[256,1408]{1,0:T(8,128)(2,1)S(1)}, bf16[256,1408]{1,0:T(8,128)(2,1)S(1)}, u32[]{:S(2)}, u32[]{:S(2)}) collective-permute-start(bf16[256,1408]{1,0:T(8,128)(2,1)S(1)} %collective-permute-done), channel_id=1, source_target_pairs={{0,28},{4,0},{8,4},{12,8},{16,12},{20,16},{24,20},{28,24},{1,29},{... | collective-permute-start | bytes 2162696 | tf_op jit(solution)/shard_map/ppermute | solution.py:21
  136.9 22.9 %collective-permute-done.1 = bf16[256,1408]{1,0:T(8,128)(2,1)S(1)} collective-permute-done((bf16[256,1408]{1,0:T(8,128)(2,1)S(1)}, bf16[256,1408]{1,0:T(8,128)(2,1)S(1)}, u32[]{:S(2)}, u32[]{:S(2)}) %collective-permute-start.1) | collective-permute-done | bytes 720928 | tf_op jit(solution)/shard_map/ppermute | solution.py:21
  160.7 5.2 %collective-permute-start.2 = (bf16[256,1408]{1,0:T(8,128)(2,1)S(1)}, bf16[256,1408]{1,0:T(8,128)(2,1)}, u32[]{:S(2)}, u32[]{:S(2)}) collective-permute-start(bf16[256,1408]{1,0:T(8,128)(2,1)S(1)} %collective-permute-done.1), channel_id=1, source_target_pairs={{0,28},{4,0},{8,4},{12,8},{16,12},{20,16},{24,20},{28,24},{1,29},{... | collective-permute-start | bytes 2162696 | tf_op jit(solution)/shard_map/ppermute | solution.py:21
  165.9 23.9 %collective-permute-done.2 = bf16[256,1408]{1,0:T(8,128)(2,1)} collective-permute-done((bf16[256,1408]{1,0:T(8,128)(2,1)S(1)}, bf16[256,1408]{1,0:T(8,128)(2,1)}, u32[]{:S(2)}, u32[]{:S(2)}) %collective-permute-start.2) | collective-permute-done | bytes 720928 | tf_op jit(solution)/shard_map/ppermute | solution.py:21
  189.7 5.3 %collective-permute-start.3 = (bf16[256,1408]{1,0:T(8,128)(2,1)}, bf16[256,1408]{1,0:T(8,128)(2,1)}, u32[]{:S(2)}, u32[]{:S(2)}) collective-permute-start(bf16[256,1408]{1,0:T(8,128)(2,1)} %collective-permute-done.2), channel_id=1, source_target_pairs={{0,28},{4,0},{8,4},{12,8},{16,12},{20,16},{24,20},{28,24},{1,29},{... | collective-permute-start | bytes 2162696 | tf_op jit(solution)/shard_map/ppermute | solution.py:21
  195.8 29.4 %collective-permute-done.3 = bf16[256,1408]{1,0:T(8,128)(2,1)} collective-permute-done((bf16[256,1408]{1,0:T(8,128)(2,1)}, bf16[256,1408]{1,0:T(8,128)(2,1)}, u32[]{:S(2)}, u32[]{:S(2)}) %collective-permute-start.3) | collective-permute-done | bytes 720928 | tf_op jit(solution)/shard_map/ppermute | solution.py:21
  225.2 5.2 %collective-permute-start.4 = (bf16[256,1408]{1,0:T(8,128)(2,1)}, bf16[256,1408]{1,0:T(8,128)(2,1)S(1)}, u32[]{:S(2)}, u32[]{:S(2)}) collective-permute-start(bf16[256,1408]{1,0:T(8,128)(2,1)} %collective-permute-done.3), channel_id=1, source_target_pairs={{0,28},{4,0},{8,4},{12,8},{16,12},{20,16},{24,20},{28,24},{1,29},{... | collective-permute-start | bytes 2162696 | tf_op jit(solution)/shard_map/ppermute | solution.py:21
  234.3 26.6 %collective-permute-done.4 = bf16[256,1408]{1,0:T(8,128)(2,1)S(1)} collective-permute-done((bf16[256,1408]{1,0:T(8,128)(2,1)}, bf16[256,1408]{1,0:T(8,128)(2,1)S(1)}, u32[]{:S(2)}, u32[]{:S(2)}) %collective-permute-start.4) | collective-permute-done | bytes 720928 | tf_op jit(solution)/shard_map/ppermute | solution.py:21
  260.9 5.1 %collective-permute-start.5 = (bf16[256,1408]{1,0:T(8,128)(2,1)S(1)}, bf16[256,1408]{1,0:T(8,128)(2,1)}, u32[]{:S(2)}, u32[]{:S(2)}) collective-permute-start(bf16[256,1408]{1,0:T(8,128)(2,1)S(1)} %collective-permute-done.4), channel_id=1, source_target_pairs={{0,28},{4,0},{8,4},{12,8},{16,12},{20,16},{24,20},{28,24},{1,29},{... | collective-permute-start | bytes 2162696 | tf_op jit(solution)/shard_map/ppermute | solution.py:21
  270.9 14.6 %collective-permute-done.5 = bf16[256,1408]{1,0:T(8,128)(2,1)} collective-permute-done((bf16[256,1408]{1,0:T(8,128)(2,1)S(1)}, bf16[256,1408]{1,0:T(8,128)(2,1)}, u32[]{:S(2)}, u32[]{:S(2)}) %collective-permute-start.5) | collective-permute-done | bytes 720928 | tf_op jit(solution)/shard_map/ppermute | solution.py:21
  285.6 5.3 %collective-permute-start.6 = (bf16[256,1408]{1,0:T(8,128)(2,1)}, bf16[256,1408]{1,0:T(8,128)(2,1)}, u32[]{:S(2)}, u32[]{:S(2)}) collective-permute-start(bf16[256,1408]{1,0:T(8,128)(2,1)} %collective-permute-done.5), channel_id=1, source_target_pairs={{0,28},{4,0},{8,4},{12,8},{16,12},{20,16},{24,20},{28,24},{1,29},{... | collective-permute-start | bytes 2162696 | tf_op jit(solution)/shard_map/ppermute | solution.py:21
  290.9 2.1 constant_dynamic-update-slice_fusion.10
  294.0 6.1 %psum.15 = f32[128]{0:T(128)S(1)} all-reduce(f32[128]{0:T(128)S(1)} %fusion.30), channel_id=1, replica_groups=mesh['sp'=8,'tp'=4] {'tp'}, use_global_device_ids=true, to_apply=%region_12.13 | all-reduce | flops 128 | bytes 1024 | tf_op jit(solution)/shard_map/psum | solution.py:171
  301.1 7.8 %all_gather.41 = bf16[128,2048]{1,0:T(8,128)(2,1)} all-gather(bf16[128,512]{1,0:T(8,128)(2,1)S(1)} %fusion.32), channel_id=1, replica_groups=mesh['sp'=8,'tp'=4] {'tp'}, dimensions={1}, use_global_device_ids=true | all-gather | bytes 655360 | tf_op jit(solution)/shard_map/all_gather | solution.py:176
  308.9 4.9 %collective-permute-done.6 = bf16[256,1408]{1,0:T(8,128)(2,1)} collective-permute-done((bf16[256,1408]{1,0:T(8,128)(2,1)}, bf16[256,1408]{1,0:T(8,128)(2,1)}, u32[]{:S(2)}, u32[]{:S(2)}) %collective-permute-start.6) | collective-permute-done | bytes 720928 | tf_op jit(solution)/shard_map/ppermute | solution.py:21
  319.8 2.1 constant_dynamic-update-slice_fusion.5
  321.9 2.1 constant_dynamic-update-slice_fusion.4
  326.0 2.1 constant_dynamic-update-slice_fusion.2
  328.1 2.1 constant_dynamic-update-slice_fusion.1
  330.2 4.7 %fusion.75 = f32[128,1408]{1,0:T(8,128)} fusion(bf16[128,2048]{1,0:T(8,128)(2,1)} %all_gather.41, bf16[2048,1408]{1,0:T(8,128)(2,1)} %all-gather.9.cloned.1.call-done), kind=kOutput, calls=%fused_computation.137 | convolution fusion | flops 738197504 | bytes 7012352 | tf_op jit(solution)/shard_map/dot_general | solution.py:178
  334.8 51.8 %all-gather.11.cloned.1.call-done = bf16[1408,2048]{1,0:T(8,128)(2,1)} async-done(((bf16[1408,256]{1,0:T(8,128)(2,1)}), bf16[1408,2048]{1,0:T(8,128)(2,1)}) %all-gather.11.cloned.1.call-update) | async-done | bytes 5767184 | tf_op jit(solution)/shard_map/all_gather | solution.py:109
  386.7 7.2 %convolution_convert_fusion.1 = bf16[128,2048]{1,0:T(8,128)(2,1)} fusion(bf16[1408,2048]{1,0:T(8,128)(2,1)} %all-gather.11.cloned.1.call-done, f32[128,1408]{1,0:T(8,128)} %fusion.75, bf16[128,2048]{1,0:T(8,128)(2,1)S(1)} %copy-done.5, bf16[4096,1408]{1,0:T(8,128)(2,1)} %constant_dynamic-update-slice_fusion.1, s32[]{:T(128)S(6)} %select_n.87), kind=kOutput, calls=%fused_computation.40 | convolution fusion | flops 1477738496 | bytes 13303812 | tf_op jit(solution)/shard_map/dot_general | solution.py:180
  393.9 20.0 %reduce-scatter.5.cloned.1.call-done = bf16[128,512]{1,0:T(8,128)(2,1)} async-done(((bf16[128,2048]{1,0:T(8,128)(2,1)}), bf16[128,512]{1,0:T(8,128)(2,1)}) %reduce-scatter.5.cloned.1.call-update) | async-done | bytes 131088 | tf_op jit(solution)/shard_map/reduce_scatter | solution.py:181
  (146 shorter events, 74.1 us)
Async XLA Ops:
  6.5 104.1 %copy-start = (bf16[512,2048]{1,0:T(8,128)(2,1)S(1)}, bf16[512,2048]{1,0:T(8,128)(2,1)}, u32[]{:S(2)}) copy-start(bf16[512,2048]{1,0:T(8,128)(2,1)} %param.25) | copy-start | bytes 6291460
  6.5 66.1 %all-gather.13.cloned.1.call-start = ((), (), s32[]{:S(2)}) async-start(), calls=%async_computation.6 | async-start | bytes 2359296 | tf_op jit(solution)/shard_map/all_gather | solution.py:29
  19.9 0.7 copy-start.1
  19.9 94.4 %copy-start.2 = (bf16[256,1408]{1,0:T(8,128)(2,1)S(1)}, bf16[256,1408]{1,0:T(8,128)(2,1)}, u32[]{:S(2)}) copy-start(bf16[256,1408]{1,0:T(8,128)(2,1)} %param.27) | copy-start | bytes 2162692
  20.6 272.3 %reduce-scatter.3.cloned.1.call-start = ((), (), s32[]{:S(2)}) async-start(), calls=%async_computation.2 | async-start | bytes 655360 | tf_op jit(solution)/shard_map/reduce_scatter | solution.py:166
  65.1 7.5 %copy-start.8 = (pred[64,64]{0,1:T(8,128)(4,1)}, pred[64,64]{0,1:T(8,128)(4,1)S(1)}, u32[]{:S(2)}) copy-start(pred[64,64]{0,1:T(8,128)(4,1)S(1)} %iota_compare_fusion) | copy-start | bytes 12292
  96.4 4.7 %copy-start.9 = (f32[2,2]{0,1:T(2,128)}, f32[2,2]{0,1:T(2,128)S(1)}, u32[]{:S(2)}) copy-start(f32[2,2]{0,1:T(2,128)S(1)} %fusion.65) | copy-start | bytes 52
  112.9 217.3 %all-gather.9.cloned.1.call-start = ((), (), s32[]{:S(2)}) async-start(), calls=%async_computation.3 | async-start | bytes 6488064 | tf_op jit(solution)/shard_map/all_gather | solution.py:108
  113.7 273.0 %all-gather.11.cloned.1.call-start = ((), (), s32[]{:S(2)}) async-start(), calls=%async_computation.4 | async-start | bytes 6488064 | tf_op jit(solution)/shard_map/all_gather | solution.py:109
  114.2 299.7 %reduce-scatter.5.cloned.1.call-start = ((), (), s32[]{:S(2)}) async-start(), calls=%async_computation.5 | async-start | bytes 655360 | tf_op jit(solution)/shard_map/reduce_scatter | solution.py:181
  114.3 18.0 %collective-permute-start = (bf16[256,1408]{1,0:T(8,128)(2,1)S(1)}, bf16[256,1408]{1,0:T(8,128)(2,1)S(1)}, u32[]{:S(2)}, u32[]{:S(2)}) collective-permute-start(bf16[256,1408]{1,0:T(8,128)(2,1)S(1)} %copy-done.2), channel_id=1, source_target_pairs={{0,28},{4,0},{8,4},{12,8},{16,12},{20,16},{24,20},{28,24},{1,29},{... | collective-permute-start | bytes 2162696 | tf_op jit(solution)/shard_map/ppermute | solution.py:21
  132.2 27.5 %collective-permute-start.1 = (bf16[256,1408]{1,0:T(8,128)(2,1)S(1)}, bf16[256,1408]{1,0:T(8,128)(2,1)S(1)}, u32[]{:S(2)}, u32[]{:S(2)}) collective-permute-start(bf16[256,1408]{1,0:T(8,128)(2,1)S(1)} %collective-permute-done), channel_id=1, source_target_pairs={{0,28},{4,0},{8,4},{12,8},{16,12},{20,16},{24,20},{28,24},{1,29},{... | collective-permute-start | bytes 2162696 | tf_op jit(solution)/shard_map/ppermute | solution.py:21
  159.8 0.9 copy-start.3
  160.7 29.0 %collective-permute-start.2 = (bf16[256,1408]{1,0:T(8,128)(2,1)S(1)}, bf16[256,1408]{1,0:T(8,128)(2,1)}, u32[]{:S(2)}, u32[]{:S(2)}) collective-permute-start(bf16[256,1408]{1,0:T(8,128)(2,1)S(1)} %collective-permute-done.1), channel_id=1, source_target_pairs={{0,28},{4,0},{8,4},{12,8},{16,12},{20,16},{24,20},{28,24},{1,29},{... | collective-permute-start | bytes 2162696 | tf_op jit(solution)/shard_map/ppermute | solution.py:21
  189.7 35.5 %collective-permute-start.3 = (bf16[256,1408]{1,0:T(8,128)(2,1)}, bf16[256,1408]{1,0:T(8,128)(2,1)}, u32[]{:S(2)}, u32[]{:S(2)}) collective-permute-start(bf16[256,1408]{1,0:T(8,128)(2,1)} %collective-permute-done.2), channel_id=1, source_target_pairs={{0,28},{4,0},{8,4},{12,8},{16,12},{20,16},{24,20},{28,24},{1,29},{... | collective-permute-start | bytes 2162696 | tf_op jit(solution)/shard_map/ppermute | solution.py:21
  225.2 35.7 %collective-permute-start.4 = (bf16[256,1408]{1,0:T(8,128)(2,1)}, bf16[256,1408]{1,0:T(8,128)(2,1)S(1)}, u32[]{:S(2)}, u32[]{:S(2)}) collective-permute-start(bf16[256,1408]{1,0:T(8,128)(2,1)} %collective-permute-done.3), channel_id=1, source_target_pairs={{0,28},{4,0},{8,4},{12,8},{16,12},{20,16},{24,20},{28,24},{1,29},{... | collective-permute-start | bytes 2162696 | tf_op jit(solution)/shard_map/ppermute | solution.py:21
  260.9 9.1 %copy-start.4 = (bf16[256,1408]{1,0:T(8,128)(2,1)}, bf16[256,1408]{1,0:T(8,128)(2,1)S(1)}, u32[]{:S(2)}) copy-start(bf16[256,1408]{1,0:T(8,128)(2,1)S(1)} %collective-permute-done.4) | copy-start | bytes 2162692
  260.9 24.7 %collective-permute-start.5 = (bf16[256,1408]{1,0:T(8,128)(2,1)S(1)}, bf16[256,1408]{1,0:T(8,128)(2,1)}, u32[]{:S(2)}, u32[]{:S(2)}) collective-permute-start(bf16[256,1408]{1,0:T(8,128)(2,1)S(1)} %collective-permute-done.4), channel_id=1, source_target_pairs={{0,28},{4,0},{8,4},{12,8},{16,12},{20,16},{24,20},{28,24},{1,29},{... | collective-permute-start | bytes 2162696 | tf_op jit(solution)/shard_map/ppermute | solution.py:21
  285.6 28.3 %collective-permute-start.6 = (bf16[256,1408]{1,0:T(8,128)(2,1)}, bf16[256,1408]{1,0:T(8,128)(2,1)}, u32[]{:S(2)}, u32[]{:S(2)}) collective-permute-start(bf16[256,1408]{1,0:T(8,128)(2,1)} %collective-permute-done.5), channel_id=1, source_target_pairs={{0,28},{4,0},{8,4},{12,8},{16,12},{20,16},{24,20},{28,24},{1,29},{... | collective-permute-start | bytes 2162696 | tf_op jit(solution)/shard_map/ppermute | solution.py:21
  316.8 69.9 %copy-start.5 = (bf16[128,2048]{1,0:T(8,128)(2,1)S(1)}, bf16[128,2048]{1,0:T(8,128)(2,1)}, u32[]{:S(2)}) copy-start(bf16[128,2048]{1,0:T(8,128)(2,1)} %all_gather.41) | copy-start | bytes 1572868
  328.1 85.8 %copy-start.6 = (bf16[128,512]{1,0:T(8,128)(2,1)S(1)}, bf16[128,512]{1,0:T(8,128)(2,1)}, u32[]{:S(2)}) copy-start(bf16[128,512]{1,0:T(8,128)(2,1)} %param.17) | copy-start | bytes 393220
  328.1 85.8 %copy-start.7 = (bf16[128,512]{1,0:T(8,128)(2,1)S(1)}, bf16[128,512]{1,0:T(8,128)(2,1)}, u32[]{:S(2)}) copy-start(bf16[128,512]{1,0:T(8,128)(2,1)} %reduce-scatter.3.cloned.1.call-done) | copy-start | bytes 393220
Sparse Core Ops, SparseCore 0:
  20.7 51.9 all-gather.12
  113.0 20.5 reduce-scatter.2
  135.8 144.3 all-gather.8
  282.1 104.5 all-gather.10
  394.1 19.7 reduce-scatter.4
